TPU v7x, 32 devices: a whole 2x2x4 slice. The times are simulated.
32 devices in a mesh: rep: 2 (over y), fs: 4 (over z), tp: 4 (over x, core).
Axes of the slice: x: 2, y: 2, z: 4, core: 2. Of those that a mesh axis runs over, the one named last changes fastest.
Arguments:
- tokens: bfloat16 [2048, 2048], P(('rep', 'fs')), may hold values from -6 to 6
- gate_weight: bfloat16 [2048, 2816], P('fs', 'tp'), may hold values from -0.125 to 0.125
- up_weight: bfloat16 [2048, 2816], P('fs', 'tp'), may hold values from -0.125 to 0.125
- down_weight: bfloat16 [2816, 2048], P('tp', 'fs'), may hold values from -0.109375 to 0.109375
- out_grad: bfloat16 [2048, 2048], P(('rep', 'fs')), may hold values from -6 to 6
Outputs:
- input_grad: bfloat16 [2048, 2048], P(('rep', 'fs'))
- down_grad: float32 [2816, 2048], P('tp', 'fs')
- row_norms: float32 [2816], P('tp')
All inputs are finite; a program needn't handle non-finite values.
Results may differ from a plain program's by a relative error of at most 0.024.
Values may be sent and summed in bfloat16 or wider, within the bound.
A program may use at most 64 MiB of HBM per device.

v0:
```python
import jax
import jax.numpy as jnp
from jax import lax
from jax.sharding import PartitionSpec as P


def contract_last(left, right):
    return lax.dot_general(
        left, right, (((1,), (1,)), ((), ())), preferred_element_type=jnp.float32
    )


def contract_first(left, right):
    return lax.dot_general(
        left, right, (((0,), (0,)), ((), ())), preferred_element_type=jnp.float32
    )


def on_device(tokens, gate_weight, up_weight, down_weight, out_grad):
    down_full = lax.all_gather(down_weight, "fs", axis=1, tiled=True)
    gate_full, up_full = (
        lax.all_gather(gate_weight, "fs", axis=0, tiled=True),
        lax.all_gather(up_weight, "fs", axis=0, tiled=True),
    )
    gate_pre = jnp.dot(tokens, gate_full, preferred_element_type=jnp.float32)
    up_pre = jnp.dot(tokens, up_full, preferred_element_type=jnp.float32)
    sigma = jax.nn.sigmoid(gate_pre)
    activated = gate_pre * sigma
    hidden = (activated * up_pre).astype(jnp.bfloat16)
    hid_grad = contract_last(out_grad, down_full)
    up_grad = (hid_grad * activated).astype(jnp.bfloat16)
    gate_grad = (hid_grad * up_pre * sigma * (1.0 + gate_pre * (1.0 - sigma))).astype(jnp.bfloat16)
    partial_value = contract_last(gate_grad, gate_full) + contract_last(up_grad, up_full)
    input_grad = lax.psum(partial_value.astype(jnp.bfloat16), "tp")
    columns = lax.all_to_all(out_grad, "fs", split_axis=1, concat_axis=0, tiled=True)
    shard = contract_first(lax.all_gather(hidden, "fs", axis=0, tiled=True), columns)
    shard = lax.psum(shard.astype(jnp.bfloat16), "rep").astype(jnp.float32)
    norms = lax.psum(jnp.sum(shard * shard, axis=1), "fs")
    return (input_grad, shard, norms)


def solution(mesh):
    return jax.shard_map(
        on_device,
        mesh=mesh,
        in_specs=(
            P(("rep", "fs"), None),
            P("fs", "tp"),
            P("fs", "tp"),
            P("tp", "fs"),
            P(("rep", "fs"), None),
        ),
        out_specs=(P(("rep", "fs"), None), P("tp", "fs"), P("tp")),
        check_vma=False,
    )
```

profile of v0, /device:TPU:0, one launch (start us, length us, event | category | flops | bytes accessed | tf_op | source)
XLA Modules:
  0.0 329.1 jit_solution(854777100918134661)
XLA Ops:
  7.2 0.0 copy-start
  7.2 0.0 all-gather.9.cloned.1.call-start
  7.2 0.7 all-gather.9.cloned.1.call-update
  7.9 0.0 all-gather.7.cloned.1.call-start
  8.0 0.7 all-gather.7.cloned.1.call-update
  8.7 0.0 all-gather.5.cloned.1.call-start
  8.7 0.7 all-gather.5.cloned.1.call-update
  9.4 0.0 all-gather.11.cloned.1.call-start
  9.4 62.0 %all-gather.9.cloned.1.call-done = bf16[2048,704]{0,1:T(8,128)(2,1)} async-done(((bf16[512,704]{0,1:T(8,128)(2,1)}), bf16[2048,704]{0,1:T(8,128)(2,1)}) %all-gather.9.cloned.1.call-update) | async-done | bytes 2883600 | tf_op jit(solution)/shard_map/all_gather | solution.py:22
  71.4 2.8 fusion.8
  74.2 0.0 copy-start.3
  74.2 56.6 %all-gather.7.cloned.1.call-done = bf16[2048,704]{0,1:T(8,128)(2,1)} async-done(((bf16[512,704]{0,1:T(8,128)(2,1)}), bf16[2048,704]{0,1:T(8,128)(2,1)}) %all-gather.7.cloned.1.call-update) | async-done | bytes 2883600 | tf_op jit(solution)/shard_map/all_gather | solution.py:23
  130.8 3.7 %multiply_convert_fusion = (bf16[256,704]{0,1:T(8,128)(2,1)}, f32[256,704]{0,1:T(8,128)}) fusion(f32[256,704]{0,1:T(8,128)S(1)} %fusion.8, bf16[256,2048]{1,0:T(8,128)(2,1)S(1)} %copy-done, bf16[2048,704]{0,1:T(8,128)(2,1)} %all-gather.7.cloned.1.call-done), kind=kOutput, calls=%fused_computation.4 | convolution fusion | flops 739278848 | bytes 5734400 | tf_op jit(solution)/shard_map/dot_general | solution.py:26
  134.6 0.0 all-gather.11.cloned.1.call-update
  134.6 0.0 all-reduce.5.cloned.1.call-start
  134.7 0.5 copy.8
  135.2 56.6 %all_to_all.19 = bf16[256,4,512]{0,2,1:T(8,128)(2,1)S(1)} all-to-all(bf16[256,4,512]{0,2,1:T(8,128)(2,1)S(1)} %bitcast.14), channel_id=1, replica_groups=mesh['rep'=2,'fs'=4,'tp'=4] {'fs'}, dimensions={1} | all-to-all | bytes 2097152 | tf_op jit(solution)/shard_map/all_to_all | solution.py:35
  191.8 0.5 copy.9
  192.4 17.8 %all-gather.5.cloned.1.call-done = bf16[704,2048]{1,0:T(8,128)(2,1)} async-done(((bf16[704,512]{1,0:T(8,128)(2,1)}), bf16[704,2048]{1,0:T(8,128)(2,1)}) %all-gather.5.cloned.1.call-update) | async-done | bytes 2883600 | tf_op jit(solution)/shard_map/all_gather | solution.py:20
  210.1 3.9 %fusion.7 = f32[256,704]{0,1:T(8,128)} fusion(bf16[256,2048]{1,0:T(8,128)(2,1)} %param.9, bf16[704,2048]{1,0:T(8,128)(2,1)} %all-gather.5.cloned.1.call-done), kind=kOutput, calls=%fused_computation.13 | convolution fusion | flops 738197504 | bytes 4653056 | tf_op jit(solution)/shard_map/dot_general | solution.py:8
  214.1 32.2 %all-gather.11.cloned.1.call-done = bf16[1024,704]{0,1:T(8,128)(2,1)} async-done(((bf16[256,704]{0,1:T(8,128)(2,1)}), bf16[1024,704]{0,1:T(8,128)(2,1)}) %all-gather.11.cloned.1.call-update) | async-done | bytes 1441808 | tf_op jit(solution)/shard_map/all_gather | solution.py:36
  246.3 3.2 convolution_convert_fusion
  249.5 0.0 all-reduce.5.cloned.1.call-update
  249.5 0.0 all-reduce.3.cloned.1.call-start
  249.6 3.5 %fusion.2 = f32[256,2048]{1,0:T(8,128)S(1)} fusion(bf16[2048,704]{0,1:T(8,128)(2,1)} %all-gather.9.cloned.1.call-done, f32[256,704]{0,1:T(8,128)S(1)} %copy-done.4, f32[256,704]{0,1:T(8,128)} %fusion.7, f32[256,704]{0,1:T(8,128)} %get-tuple-element.6), kind=kOutput, calls=%fused_computation.9 | convolution fusion | flops 739999744 | bytes 7143424 | tf_op jit(solution)/shard_map/dot_general | solution.py:8
  253.1 2.0 fusion
  255.2 0.0 all-reduce.3.cloned.1.call-update
  255.2 25.6 %all-reduce.5.cloned.1.call-done = bf16[704,512]{1,0:T(8,128)(2,1)} async-done(((bf16[704,512]{1,0:T(8,128)(2,1)}), bf16[704,512]{1,0:T(8,128)(2,1)}) %all-reduce.5.cloned.1.call-update) | async-done | bytes 720912 | tf_op jit(solution)/shard_map/psum | solution.py:37
  280.8 2.3 multiply_reduce_fusion
  283.1 12.2 %psum.23 = f32[704]{0:T(1024)} all-reduce(f32[704]{0:T(1024)S(1)} %get-tuple-element.3), channel_id=1, replica_groups=mesh['rep'=2,'fs'=4,'tp'=4] {'fs'}, use_global_device_ids=true, to_apply=%region_3.0 | all-reduce | flops 704 | bytes 5632 | tf_op jit(solution)/shard_map/psum | solution.py:38
  295.4 24.5 %all-reduce.3.cloned.1.call-done = bf16[256,2048]{1,0:T(8,128)(2,1)} async-done(((bf16[256,2048]{1,0:T(8,128)(2,1)}), bf16[256,2048]{1,0:T(8,128)(2,1)}) %all-reduce.3.cloned.1.call-update) | async-done | bytes 1048592 | tf_op jit(solution)/shard_map/psum | solution.py:34
  319.9 2.3 copy.12
  (10 shorter events, 0.0 us)
Async XLA Ops:
  7.2 64.3 %copy-start = (bf16[256,2048]{1,0:T(8,128)(2,1)S(1)}, bf16[256,2048]{1,0:T(8,128)(2,1)}, u32[]{:S(2)}) copy-start(bf16[256,2048]{1,0:T(8,128)(2,1)} %param.5) | copy-start | bytes 3145732
  7.2 64.2 %all-gather.9.cloned.1.call-start = ((), (), s32[]{:S(2)}) async-start(), calls=%async_computation.3 | async-start | bytes 3604480 | tf_op jit(solution)/shard_map/all_gather | solution.py:22
  7.9 122.9 %all-gather.7.cloned.1.call-start = ((), (), s32[]{:S(2)}) async-start(), calls=%async_computation.2 | async-start | bytes 3604480 | tf_op jit(solution)/shard_map/all_gather | solution.py:23
  8.7 201.5 %all-gather.5.cloned.1.call-start = ((), (), s32[]{:S(2)}) async-start(), calls=%async_computation.1 | async-start | bytes 3604480 | tf_op jit(solution)/shard_map/all_gather | solution.py:20
  9.4 236.9 %all-gather.11.cloned.1.call-start = ((), (), s32[]{:S(2)}) async-start(), calls=%async_computation.5 | async-start | bytes 1802240 | tf_op jit(solution)/shard_map/all_gather | solution.py:36
  74.2 60.4 %copy-start.3 = (f32[256,704]{0,1:T(8,128)}, f32[256,704]{0,1:T(8,128)S(1)}, u32[]{:S(2)}) copy-start(f32[256,704]{0,1:T(8,128)S(1)} %fusion.8) | copy-start | bytes 2162692
  74.2 60.4 %copy-start.2 = (bf16[256,2048]{1,0:T(8,128)(2,1)S(1)}, bf16[256,2048]{1,0:T(8,128)(2,1)}, u32[]{:S(2)}) copy-start(bf16[256,2048]{1,0:T(8,128)(2,1)} %param.9) | copy-start | bytes 3145732
  134.6 146.2 %all-reduce.5.cloned.1.call-start = ((), (), s32[]{:S(2)}) async-start(), calls=%async_computation.6 | async-start | bytes 1441792 | tf_op jit(solution)/shard_map/psum | solution.py:37
  246.3 3.3 %copy-start.4 = (f32[256,704]{0,1:T(8,128)S(1)}, f32[256,704]{0,1:T(8,128)}, u32[]{:S(2)}) copy-start(f32[256,704]{0,1:T(8,128)} %copy-done.3) | copy-start | bytes 2162692
  249.5 70.4 %all-reduce.3.cloned.1.call-start = ((), (), s32[]{:S(2)}) async-start(), calls=%async_computation.4 | async-start | bytes 2097152 | tf_op jit(solution)/shard_map/psum | solution.py:34
  249.6 3.5 %copy-start.1 = (bf16[2048,704]{0,1:T(8,128)(2,1)S(1)}, bf16[2048,704]{0,1:T(8,128)(2,1)}, u32[]{:S(2)}) copy-start(bf16[2048,704]{0,1:T(8,128)(2,1)} %all-gather.7.cloned.1.call-done) | copy-start | bytes 8650756
  249.6 3.5 %copy-start.5 = (f32[256,704]{0,1:T(8,128)S(1)}, f32[256,704]{0,1:T(8,128)}, u32[]{:S(2)}) copy-start(f32[256,704]{0,1:T(8,128)} %fusion.7) | copy-start | bytes 2162692
Sparse Core Ops, SparseCore 0:
  9.6 61.8 all-gather.8
  73.0 57.7 all-gather.6
  132.4 77.6 all-gather.4
  211.6 34.6 all-gather.10
  249.6 31.1 all-reduce.4
  283.6 36.2 all-reduce.2
where the time goes:
time: 329 us
  waiting for transfers between devices  221 us (67%)
  blocking collectives  68.9 us (21%)
  matrix products  19.2 us (6%)
  between operations  14.2 us (4%)
  local copies, waits for them, and re-layouts  3.4 us (1%)
    all_gather x1, waiting for transfers between devices, on_device(): lax.all_gather(gate_weight, 'fs', axis=0, tiled=True)  62 us
    all_to_all x1, blocking collectives, on_device(): lax.all_to_all(out_grad, 'fs', split_axis=1, concat_axis=0, tiled=True)  56.6 us
    all_gather x1, waiting for transfers between devices, on_device(): lax.all_gather(up_weight, 'fs', axis=0, tiled=True)  56.6 us
    all_gather x1, waiting for transfers between devices, on_device(): lax.all_gather(hidden, 'fs', axis=0, tiled=True)  32.2 us
    psum x1, waiting for transfers between devices, on_device(): shard = lax.psum(shard.astype(jnp.bfloat16), 'rep').astype(jnp.float32)  25.6 us
    psum x1, waiting for transfers between devices, on_device(): input_grad = lax.psum(partial_value.astype(jnp.bfloat16), 'tp')  24.5 us
    all_gather x1, waiting for transfers between devices, on_device(): down_full = lax.all_gather(down_weight, 'fs', axis=1, tiled=True)  17.8 us
    psum x1, blocking collectives, on_device(): norms = lax.psum(jnp.sum(shard * shard, axis=1), 'fs')  12.2 us
  transfers between devices with their start and end apart: 6, of which 6 were waited for; matrix products, arithmetic and copies ran while one was open for 6% of the time, Pallas kernels for 0%

commit v1 on v0

--- a/solution.py
+++ b/solution.py
@@ -32,7 +32,10 @@
     gate_grad = (hid_grad * up_pre * sigma * (1.0 + gate_pre * (1.0 - sigma))).astype(jnp.bfloat16)
     partial_value = contract_last(gate_grad, gate_full) + contract_last(up_grad, up_full)
     input_grad = lax.psum(partial_value.astype(jnp.bfloat16), "tp")
-    columns = lax.all_to_all(out_grad, "fs", split_axis=1, concat_axis=0, tiled=True)
+    columns = jnp.concatenate(
+        lax.all_to_all(jnp.stack(jnp.split(out_grad, lax.axis_size("fs"), axis=1)), "fs", 0, 0),
+        axis=0,
+    )
     shard = contract_first(lax.all_gather(hidden, "fs", axis=0, tiled=True), columns)
     shard = lax.psum(shard.astype(jnp.bfloat16), "rep").astype(jnp.float32)
     norms = lax.psum(jnp.sum(shard * shard, axis=1), "fs")

time: 329 us -> 331 us (level)
  blocking collectives: 68.9 us -> 12.2 us
  waiting for transfers between devices: 221 us -> 276 us
  starting transfers between devices: 0.24 us -> 3.77 us
    all_to_all x1 -> x0, blocking collectives: 56.6 us -> none  [on_device(): lax.all_to_all(out_grad, 'fs', split_axis=1, concat_axis=0, tiled=True)]
    all_gather x1, waiting for transfers between devices: 17.8 us -> 72.4 us  [on_device(): down_full = lax.all_gather(down_weight, 'fs', axis=1, tiled=True)]
    all_to_all x0 -> x1, starting transfers between devices: none -> 3.54 us  [on_device(): lax.all_to_all(jnp.stack(jnp.split(out_grad, lax.axis_size('fs'), axis=1)...]
  transfers between devices with their start and end apart: 6 -> 7, of which waited for: 6 -> 6; matrix products, arithmetic and copies ran while one was open for 6% -> 6% of each run, Pallas kernels for 0% -> 0%
where the time goes in v1:
time: 331 us
  waiting for transfers between devices  276 us (83%)
  matrix products  18.9 us (6%)
  between operations  14.2 us (4%)
  blocking collectives  12.2 us (4%)
  starting transfers between devices  3.77 us (1%)
  other arithmetic  3.45 us (1%)
    all_gather x1, waiting for transfers between devices, on_device(): down_full = lax.all_gather(down_weight, 'fs', axis=1, tiled=True)  72.4 us
    all_gather x1, waiting for transfers between devices, on_device(): lax.all_gather(gate_weight, 'fs', axis=0, tiled=True)  62 us
    all_gather x1, waiting for transfers between devices, on_device(): lax.all_gather(up_weight, 'fs', axis=0, tiled=True)  56.6 us
    all_gather x1, waiting for transfers between devices, on_device(): lax.all_gather(hidden, 'fs', axis=0, tiled=True)  32.5 us
    psum x1, waiting for transfers between devices, on_device(): shard = lax.psum(shard.astype(jnp.bfloat16), 'rep').astype(jnp.float32)  25.6 us
    psum x1, waiting for transfers between devices, on_device(): input_grad = lax.psum(partial_value.astype(jnp.bfloat16), 'tp')  24.5 us
    psum x1, blocking collectives, on_device(): norms = lax.psum(jnp.sum(shard * shard, axis=1), 'fs')  12.2 us
    dot_general x3, matrix products, contract_last(): lax.dot_general(left, right, (((1,), (1,)), ((), ())), preferred_element_...  9.2 us
  transfers between devices with their start and end apart: 7, of which 6 were waited for; matrix products, arithmetic and copies ran while one was open for 6% of the time, Pallas kernels for 0%

profile of v1, /device:TPU:0, one launch (start us, length us, event | category | flops | bytes accessed | tf_op | source)
XLA Modules:
  0.0 330.8 jit_solution(15749701673615155505)
XLA Ops:
  7.2 0.0 copy-start
  7.2 0.0 all-gather.9.cloned.1.call-start
  7.2 0.7 all-gather.9.cloned.1.call-update
  7.9 0.0 all-gather.7.cloned.1.call-start
  8.0 0.7 all-gather.7.cloned.1.call-update
  8.7 0.0 all-gather.5.cloned.1.call-start
  8.7 0.7 all-gather.5.cloned.1.call-update
  9.4 0.0 all-gather.11.cloned.1.call-start
  9.4 62.0 %all-gather.9.cloned.1.call-done = bf16[2048,704]{0,1:T(8,128)(2,1)} async-done(((bf16[512,704]{0,1:T(8,128)(2,1)}), bf16[2048,704]{0,1:T(8,128)(2,1)}) %all-gather.9.cloned.1.call-update) | async-done | bytes 2883600 | tf_op jit(solution)/shard_map/all_gather | solution.py:22
  71.4 2.8 fusion.8
  74.2 0.0 copy-start.3
  74.2 56.6 %all-gather.7.cloned.1.call-done = bf16[2048,704]{0,1:T(8,128)(2,1)} async-done(((bf16[512,704]{0,1:T(8,128)(2,1)}), bf16[2048,704]{0,1:T(8,128)(2,1)}) %all-gather.7.cloned.1.call-update) | async-done | bytes 2883600 | tf_op jit(solution)/shard_map/all_gather | solution.py:23
  130.8 3.7 %multiply_convert_fusion = (bf16[256,704]{0,1:T(8,128)(2,1)}, f32[256,704]{0,1:T(8,128)}) fusion(f32[256,704]{0,1:T(8,128)S(1)} %fusion.8, bf16[256,2048]{1,0:T(8,128)(2,1)S(1)} %copy-done, bf16[2048,704]{0,1:T(8,128)(2,1)} %all-gather.7.cloned.1.call-done), kind=kOutput, calls=%fused_computation.5 | convolution fusion | flops 739278848 | bytes 5734400 | tf_op jit(solution)/shard_map/dot_general | solution.py:26
  134.6 0.0 all-gather.11.cloned.1.call-update
  134.6 0.1 slice_bitcast_fusion.3
  134.7 1.1 pad_maximum_fusion
  135.8 3.5 %all-to-all-start = ((bf16[4,256,512]{2,1,0:T(8,128)(2,1)}), bf16[4,256,512]{2,1,0:T(8,128)(2,1)S(1)}, u32[]{:S(2)}, u32[]{:S(2)}) async-start(bf16[4,256,512]{2,1,0:T(8,128)(2,1)} %pad_maximum_fusion), calls=%async_computation | async-start | bytes 2097152 | tf_op jit(solution)/shard_map/all_to_all | solution.py:36
  139.4 0.0 all-reduce.5.cloned.1.call-start
  139.4 72.4 %all-gather.5.cloned.1.call-done = bf16[704,2048]{1,0:T(8,128)(2,1)} async-done(((bf16[704,512]{1,0:T(8,128)(2,1)}), bf16[704,2048]{1,0:T(8,128)(2,1)}) %all-gather.5.cloned.1.call-update) | async-done | bytes 2883600 | tf_op jit(solution)/shard_map/all_gather | solution.py:20
  211.8 3.7 %fusion.7 = f32[256,704]{0,1:T(8,128)} fusion(bf16[256,2048]{1,0:T(8,128)(2,1)S(1)} %copy-done.2, bf16[704,2048]{1,0:T(8,128)(2,1)} %all-gather.5.cloned.1.call-done), kind=kOutput, calls=%fused_computation.18 | convolution fusion | flops 738197504 | bytes 4653056 | tf_op jit(solution)/shard_map/dot_general | solution.py:8
  215.5 32.5 %all-gather.11.cloned.1.call-done = bf16[1024,704]{0,1:T(8,128)(2,1)} async-done(((bf16[256,704]{0,1:T(8,128)(2,1)}), bf16[1024,704]{0,1:T(8,128)(2,1)}) %all-gather.11.cloned.1.call-update) | async-done | bytes 1441808 | tf_op jit(solution)/shard_map/all_gather | solution.py:39
  248.0 3.2 convolution_convert_fusion
  251.2 0.0 all-reduce.5.cloned.1.call-update
  251.2 0.0 all-reduce.3.cloned.1.call-start
  251.3 3.5 %fusion.2 = f32[256,2048]{1,0:T(8,128)S(1)} fusion(bf16[2048,704]{0,1:T(8,128)(2,1)} %all-gather.9.cloned.1.call-done, f32[256,704]{0,1:T(8,128)S(1)} %copy-done.4, f32[256,704]{0,1:T(8,128)} %fusion.7, f32[256,704]{0,1:T(8,128)} %get-tuple-element.10), kind=kOutput, calls=%fused_computation.10 | convolution fusion | flops 739999744 | bytes 7143424 | tf_op jit(solution)/shard_map/dot_general | solution.py:8
  254.8 2.0 fusion
  256.9 0.0 all-reduce.3.cloned.1.call-update
  256.9 25.6 %all-reduce.5.cloned.1.call-done = bf16[704,512]{1,0:T(8,128)(2,1)} async-done(((bf16[704,512]{1,0:T(8,128)(2,1)}), bf16[704,512]{1,0:T(8,128)(2,1)}) %all-reduce.5.cloned.1.call-update) | async-done | bytes 720912 | tf_op jit(solution)/shard_map/psum | solution.py:40
  282.5 2.3 multiply_reduce_fusion
  284.9 12.2 %psum.23 = f32[704]{0:T(1024)} all-reduce(f32[704]{0:T(1024)S(1)} %get-tuple-element.3), channel_id=1, replica_groups=mesh['rep'=2,'fs'=4,'tp'=4] {'fs'}, use_global_device_ids=true, to_apply=%region_3.0 | all-reduce | flops 704 | bytes 5632 | tf_op jit(solution)/shard_map/psum | solution.py:41
  297.1 24.5 %all-reduce.3.cloned.1.call-done = bf16[256,2048]{1,0:T(8,128)(2,1)} async-done(((bf16[256,2048]{1,0:T(8,128)(2,1)}), bf16[256,2048]{1,0:T(8,128)(2,1)}) %all-reduce.3.cloned.1.call-update) | async-done | bytes 1048592 | tf_op jit(solution)/shard_map/psum | solution.py:34
  321.6 2.3 copy.10
  (11 shorter events, 0.0 us)
Async XLA Ops:
  7.2 64.3 %copy-start = (bf16[256,2048]{1,0:T(8,128)(2,1)S(1)}, bf16[256,2048]{1,0:T(8,128)(2,1)}, u32[]{:S(2)}) copy-start(bf16[256,2048]{1,0:T(8,128)(2,1)} %param.5) | copy-start | bytes 3145732
  7.2 64.2 %all-gather.9.cloned.1.call-start = ((), (), s32[]{:S(2)}) async-start(), calls=%async_computation.3 | async-start | bytes 3604480 | tf_op jit(solution)/shard_map/all_gather | solution.py:22
  7.9 122.9 %all-gather.7.cloned.1.call-start = ((), (), s32[]{:S(2)}) async-start(), calls=%async_computation.2 | async-start | bytes 3604480 | tf_op jit(solution)/shard_map/all_gather | solution.py:23
  8.7 203.2 %all-gather.5.cloned.1.call-start = ((), (), s32[]{:S(2)}) async-start(), calls=%async_computation.1 | async-start | bytes 3604480 | tf_op jit(solution)/shard_map/all_gather | solution.py:20
  9.4 238.6 %all-gather.11.cloned.1.call-start = ((), (), s32[]{:S(2)}) async-start(), calls=%async_computation.5 | async-start | bytes 1802240 | tf_op jit(solution)/shard_map/all_gather | solution.py:39
  74.2 60.4 %copy-start.3 = (f32[256,704]{0,1:T(8,128)}, f32[256,704]{0,1:T(8,128)S(1)}, u32[]{:S(2)}) copy-start(f32[256,704]{0,1:T(8,128)S(1)} %fusion.8) | copy-start | bytes 2162692
  74.2 60.4 %copy-start.2 = (bf16[256,2048]{1,0:T(8,128)(2,1)S(1)}, bf16[256,2048]{1,0:T(8,128)(2,1)}, u32[]{:S(2)}) copy-start(bf16[256,2048]{1,0:T(8,128)(2,1)} %param.9) | copy-start | bytes 3145732
  135.8 79.7 %all-to-all-start = ((bf16[4,256,512]{2,1,0:T(8,128)(2,1)}), bf16[4,256,512]{2,1,0:T(8,128)(2,1)S(1)}, u32[]{:S(2)}, u32[]{:S(2)}) async-start(bf16[4,256,512]{2,1,0:T(8,128)(2,1)} %pad_maximum_fusion), calls=%async_computation | async-start | bytes 2097152 | tf_op jit(solution)/shard_map/all_to_all | solution.py:36
  139.4 143.2 %all-reduce.5.cloned.1.call-start = ((), (), s32[]{:S(2)}) async-start(), calls=%async_computation.6 | async-start | bytes 1441792 | tf_op jit(solution)/shard_map/psum | solution.py:40
  248.0 3.3 copy-start.4
  251.2 70.4 %all-reduce.3.cloned.1.call-start = ((), (), s32[]{:S(2)}) async-start(), calls=%async_computation.4 | async-start | bytes 2097152 | tf_op jit(solution)/shard_map/psum | solution.py:34
  251.3 3.5 %copy-start.1 = (bf16[2048,704]{0,1:T(8,128)(2,1)S(1)}, bf16[2048,704]{0,1:T(8,128)(2,1)}, u32[]{:S(2)}) copy-start(bf16[2048,704]{0,1:T(8,128)(2,1)} %all-gather.7.cloned.1.call-done) | copy-start | bytes 8650756
  251.3 3.5 %copy-start.5 = (f32[256,704]{0,1:T(8,128)S(1)}, f32[256,704]{0,1:T(8,128)}, u32[]{:S(2)}) copy-start(f32[256,704]{0,1:T(8,128)} %fusion.7) | copy-start | bytes 2162692
Sparse Core Ops, SparseCore 0:
  9.6 61.8 all-gather.8
  73.0 57.7 all-gather.6
  132.4 79.3 all-gather.4
  213.3 34.6 all-gather.10
  251.4 31.1 all-reduce.4
  285.3 36.2 all-reduce.2
